TPU v7x, 512 devices: a whole 4x8x8 slice. The times are simulated.
512 devices in a mesh: sp: 32 (over z, x), tp: 16 (over y, core).
Axes of the slice: x: 4, y: 8, z: 8, core: 2. Of those that a mesh axis runs over, the one named last changes fastest.
Arguments:
- tokens: bfloat16 [32, 3072, 2048], P('sp', 'tp'), may hold values from -100 to 100
- norm_gain: float32 [2048], replicated, may hold values from 0.1 to 1.9
- key_weight: bfloat16 [2048, 1024], P('sp', 'tp'), may hold values from -0.125 to 0.125
- value_weight: bfloat16 [2048, 1024], P('sp', 'tp'), may hold values from -0.125 to 0.125
- cum_gate: float32 [32, 32, 3072], P('sp', None, 'tp'), may hold values from -448 to 0, as said below
- new_gate: float32 [32, 32], P('sp', 'tp'), may hold values from -448 to 0
- new_query: bfloat16 [32, 2048], P('sp', 'tp'), may hold values from -128 to 128
- new_kv: bfloat16 [32, 16, 128], P('sp', 'tp'), may hold values from -4 to 4
Outputs:
- kv_cache: bfloat16 [32, 16, 3072, 128], P('sp', 'tp')
- gate_log_cache: float32 [32, 32, 3072], P('sp', 'tp')
- read_out: bfloat16 [32, 2048], P('sp', 'tp')
Inputs may be any that keep to these rules, and one draw needn't show every extreme that they name: Along positions cum_gate never rises; new_gate is at most the last position's value of its prompt and head.
All inputs are finite; a program needn't handle non-finite values.
Results may differ from a plain program's by a relative error of at most 0.0071.
Values may be sent and summed in bfloat16 or wider, within the bound.
No kernel may reach another device: no remote copies, remote signals or barrier semaphores. Data moves between devices by JAX's collectives and lax.ppermute only.
A program may use at most 64 MiB of HBM per device.

v0:
```python
import math
import jax
import jax.numpy as jnp
from jax import lax
from jax.sharding import PartitionSpec as P

HEAD = 64


def sent_together(arrays, axis, dim, along):
    widths = [a.shape[along] for a in arrays]
    both = jnp.concatenate(arrays, axis=along)
    filled = lax.all_gather(both, axis, axis=dim, tiled=True)
    return tuple(jnp.split(filled, [sum(widths[:k]) for k in range(1, len(widths))], axis=along))


def normalize(rows, norm_gain):
    widened = rows.astype(jnp.float32)
    inv_rms = lax.rsqrt(jnp.mean(widened * widened, axis=-1, keepdims=True) + 1e-06)
    scaled = (widened * norm_gain).astype(jnp.bfloat16)
    return (scaled, inv_rms)


def per_device(tokens, norm_gain, key_weight, value_weight, cum_gate, new_gate, new_query, new_kv):
    key_rows, value_rows = sent_together((key_weight, value_weight), "sp", 0, 1)
    prompts, positions, model_width = tokens.shape
    local_width = key_rows.shape[1]
    kv_here = local_width // HEAD
    gate_here = lax.all_to_all(cum_gate, "tp", split_axis=1, concat_axis=2, tiled=True)
    both_weights = jnp.concatenate([key_rows, value_rows], axis=1)
    piece = lax.all_gather(tokens, "tp", axis=1, tiled=True)
    scaled, inv_rms = normalize(piece, norm_gain)
    flat = scaled.reshape(-1, model_width)
    product = jnp.dot(flat, both_weights, preferred_element_type=jnp.float32)
    product = product.reshape(piece.shape[0], piece.shape[1], 2 * local_width) * inv_rms
    projected = product.astype(jnp.bfloat16)
    length = projected.shape[1]
    key_heads = projected[:, :, :local_width].reshape(prompts, length, kv_here, HEAD)
    value_heads = projected[:, :, local_width:].reshape(prompts, length, kv_here, HEAD)
    cache_local_copy = jnp.transpose(
        jnp.concatenate([key_heads, value_heads], axis=3), (0, 2, 1, 3)
    )
    length = cache_local_copy.shape[2]
    heads_here = gate_here.shape[1]
    group = heads_here // kv_here
    scale_factor = 1.0 / math.sqrt(HEAD)
    keys = cache_local_copy[..., :HEAD]
    values = cache_local_copy[..., HEAD:]
    query = new_query.reshape(prompts, kv_here, group, HEAD)
    own_key = new_kv[..., :HEAD].astype(jnp.float32)
    own_value = new_kv[..., HEAD:].astype(jnp.float32)
    score = (
        jnp.einsum("skgd,sktd->skgt", query, keys, preferred_element_type=jnp.float32)
        * scale_factor
    )
    score = (
        score
        + new_gate.reshape(prompts, kv_here, group)[..., None]
        - gate_here.reshape(prompts, kv_here, group, length)
    )
    own = jnp.sum(query.astype(jnp.float32) * own_key[:, :, None, :], axis=3) * scale_factor
    top = jnp.maximum(jnp.max(score, axis=3), own)
    expo = jnp.exp(score - top[..., None])
    own_factor = jnp.exp(own - top)
    total = jnp.sum(expo, axis=3) + own_factor
    weights = expo.astype(jnp.bfloat16)
    numer = jnp.einsum("skgt,sktd->skgd", weights, values, preferred_element_type=jnp.float32)
    numer = numer + own_factor[..., None] * own_value[:, :, None, :]
    read_out = (numer / total[..., None]).reshape(prompts, heads_here * HEAD).astype(jnp.bfloat16)
    return (cache_local_copy, gate_here, read_out)


def solution(mesh):
    in_specs = (
        P("sp", "tp", None),
        P(),
        P("sp", "tp"),
        P("sp", "tp"),
        P("sp", None, "tp"),
        P("sp", "tp"),
        P("sp", "tp"),
        P("sp", "tp", None),
    )
    out_specs = (P("sp", "tp", None, None), P("sp", "tp", None), P("sp", "tp"))
    return jax.shard_map(
        per_device, mesh=mesh, in_specs=in_specs, out_specs=out_specs, check_vma=False
    )
```

profile of v0, /device:TPU:1, one launch (start us, length us, event | category | flops | bytes accessed | tf_op | source)
XLA Modules:
  0.0 119.5 jit_solution(1385193337184464676)
XLA Ops:
  7.2 0.7 all-gather.2.cloned.1.call-update
  7.9 1.4 %copy.13 = f32[1,32,192]{2,0,1:T(1,128)} copy(f32[1,32,192]{2,1,0:T(8,128)} %param.12) | data formatting | bytes 49152 | tf_op args[4]
  9.3 10.1 %all-to-all-start = ((f32[1,32,192]{2,0,1:T(1,128)}), f32[1,32,192]{2,0,1:T(1,128)S(1)}, u32[]{:S(2)}, u32[]{:S(2)}) async-start(f32[1,32,192]{2,0,1:T(1,128)} %copy.13), calls=%async_computation | async-start | bytes 65536 | tf_op jit(solution)/shard_map/all_to_all | solution.py:29
  19.4 0.7 convert_reduce_fusion
  20.1 0.1 reshape.184
  20.2 0.8 pad_maximum_fusion
  21.0 47.1 %all_gather.7 = bf16[2048,128]{1,0:T(8,128)(2,1)S(1)} all-gather(bf16[64,128]{1,0:T(8,128)(2,1)S(1)} %pad_maximum_fusion), channel_id=1, replica_groups=mesh['sp'=32,'tp'=16] {'sp'}, dimensions={0}, use_global_device_ids=true | all-gather | bytes 540672 | tf_op jit(solution)/shard_map/all_gather | solution.py:13
  68.1 0.8 bitcast_convert_fusion
  68.9 0.1 multiply_reduce_fusion
  69.0 0.5 broadcast.78
  69.5 1.3 %reduce.13 = bf16[128]{0:T(256)(128)(2,1)S(1)} reduce(bf16[1,128]{1,0:T(2,128)(2,1)} %param.14, bf16[]{:T(256)} %broadcast.78), dimensions={0}, to_apply=%param.14.reduce_sub_computation.3 | reduce | bytes 514 | tf_op args[6]
  70.8 0.1 reshape.181
  70.9 0.1 reshape.182
  71.0 0.7 all_to_all.16
  71.7 22.2 %all-gather.2.cloned.1.call-done = bf16[1,3072,2048]{2,1,0:T(8,128)(2,1)} async-done(((bf16[1,192,2048]{2,1,0:T(8,128)(2,1)}), bf16[1,3072,2048]{2,1,0:T(8,128)(2,1)}) %all-gather.2.cloned.1.call-update) | async-done | bytes 12582928 | tf_op jit(solution)/shard_map/all_gather | solution.py:31
  93.9 7.1 %fusion.1 = f32[3072]{0:T(1024)S(1)} fusion(bf16[1,3072,2048]{2,1,0:T(8,128)(2,1)} %all-gather.2.cloned.1.call-done), kind=kLoop, calls=%fused_computation.3 | loop fusion | flops 18871296 | bytes 12595200 | tf_op jit(solution)/shard_map/reduce_sum | solution.py:19
  101.1 8.9 %fusion.12 = bf16[1,3072,128]{1,2,0:T(8,128)(2,1)S(1)} fusion(bf16[2048,128]{1,0:T(8,128)(2,1)S(1)} %all_gather.7, bf16[1,3072,2048]{2,1,0:T(8,128)(2,1)} %all-gather.2.cloned.1.call-done, f32[2048]{0:T(1024)S(1)} %copy-done, f32[3072]{0:T(1024)S(1)} %add_rsqrt_fusion), kind=kOutput, calls=%fused_computation.9 | convolution fusion | flops 1630273536 | bytes 13914112 | tf_op jit(solution)/shard_map/dot_general | solution.py:34
  109.9 0.1 slice_bitcast_fusion.5
  110.0 0.1 maximum_bitcast_fusion
  110.1 1.2 copy.15
  111.2 0.3 fusion.24
  111.5 0.2 fusion.20
  111.7 0.3 fusion.19
  112.0 0.6 convert_element_type.57
  (10 shorter events, 0.1 us)
Async XLA Ops:
  7.2 93.9 %copy-start = (f32[2048]{0:T(1024)S(1)}, f32[2048]{0:T(1024)}, u32[]{:S(2)}) copy-start(f32[2048]{0:T(1024)} %param.9) | copy-start | bytes 24580
  7.2 86.8 %all-gather.2.cloned.1.call-start = ((), (), s32[]{:S(2)}) async-start(), calls=%async_computation.1 | async-start | bytes 13369344 | tf_op jit(solution)/shard_map/all_gather | solution.py:31
  9.3 61.6 %all-to-all-start = ((f32[1,32,192]{2,0,1:T(1,128)}), f32[1,32,192]{2,0,1:T(1,128)S(1)}, u32[]{:S(2)}, u32[]{:S(2)}) async-start(f32[1,32,192]{2,0,1:T(1,128)} %copy.13), calls=%async_computation | async-start | bytes 65536 | tf_op jit(solution)/shard_map/all_to_all | solution.py:29
  101.0 10.2 %copy-start.1 = (f32[1,2]{1,0:T(1,128)S(1)}, f32[1,2]{1,0:T(1,128)}, u32[]{:S(2)}) copy-start(f32[1,2]{1,0:T(1,128)} %param.13) | copy-start | bytes 28
Sparse Core Ops, SparseCore 0:
  10.1 83.7 all-gather.1
where the time goes:
time: 120 us; the launch traced here: 119 us
  blocking collectives  47.1 us (39%)
  waiting for transfers between devices  22.9 us (19%)
  between operations  14.1 us (12%)
  other arithmetic  11.1 us (9%)
  starting transfers between devices  10.2 us (8%)
  matrix products  9.43 us (8%)
  local copies, waits for them, and re-layouts  4.71 us (4%)
    all_gather x1, blocking collectives, sent_together(): filled = lax.all_gather(both, axis, axis=dim, tiled=True)  47.1 us
    all_gather x1, waiting for transfers between devices, per_device(): piece = lax.all_gather(tokens, 'tp', axis=1, tiled=True)  22.2 us
    all_to_all x1, starting transfers between devices, per_device(): lax.all_to_all(cum_gate, 'tp', split_axis=1, concat_axis=2, tiled=True)  10.1 us
    dot_general x1, matrix products, per_device(): product = jnp.dot(flat, both_weights, preferred_element_type=jnp.float32)  8.88 us
    reduce_sum x1, other arithmetic, normalize(): jnp.mean(widened * widened, axis=-1, keepdims=True) + 1e-06  7.09 us
    unnamed x7, local copies, waits for them, and re-layouts  3.09 us
  transfers between devices with their start and end apart: 2, of which 1 were waited for; matrix products, arithmetic and copies ran while one was open for 5% of the time, Pallas kernels for 0%

commit v1 on v0

--- a/solution.py
+++ b/solution.py
@@ -28,7 +28,9 @@
     kv_here = local_width // HEAD
     gate_here = lax.all_to_all(cum_gate, "tp", split_axis=1, concat_axis=2, tiled=True)
     both_weights = jnp.concatenate([key_rows, value_rows], axis=1)
-    piece = lax.all_gather(tokens, "tp", axis=1, tiled=True)
+    piece = jnp.concatenate(
+        lax.all_to_all(jnp.stack([tokens] * lax.axis_size("tp")), "tp", 0, 0), axis=1
+    )
     scaled, inv_rms = normalize(piece, norm_gain)
     flat = scaled.reshape(-1, model_width)
     product = jnp.dot(flat, both_weights, preferred_element_type=jnp.float32)

time: 120 us -> 325 us (2.71)
  waiting for transfers between devices: 22.9 us -> 223 us
  blocking collectives: 47.1 us -> 64.4 us
  between operations: 14.1 us -> 0.71 us
  local copies, waits for them, and re-layouts: 4.71 us -> 11.4 us
  starting transfers between devices: 10.2 us -> 5.2 us
  matrix products: 9.43 us -> 4.84 us
  other arithmetic: 11.1 us -> 14.6 us
    all_to_all x1, waiting for transfers between devices: 0.01 us -> 223 us  [per_device(): lax.all_to_all(jnp.stack([tokens] * lax.axis_size('tp')), 'tp', 0, 0)]
    all_gather x1 -> x0, waiting for transfers between devices: 22.2 us -> none  [per_device(): piece = lax.all_gather(tokens, 'tp', axis=1, tiled=True)]
    all_to_all x0 -> x1, blocking collectives: none -> 16.7 us  [per_device(): lax.all_to_all(cum_gate, 'tp', split_axis=1, concat_axis=2, tiled=True)]
    another operation x1 -> x2, local copies, waits for them, and re-layouts: 0.09 us -> 7.3 us  [the longest x1 7.21 us: per_device(): jnp.stack([tokens] * lax.axis_size('tp'))]
    convert_element_type x0 -> x1, other arithmetic: none -> 6.23 us  [normalize(): scaled = (widened * norm_gain).astype(jnp.bfloat16)]
    all_to_all x1, starting transfers between devices: 10.1 us -> 5.2 us  [per_device(): lax.all_to_all(jnp.stack([tokens] * lax.axis_size('tp')), 'tp', 0, 0)]
    dot_general x1, matrix products: 8.88 us -> 4.28 us  [per_device(): product = jnp.dot(flat, both_weights, preferred_element_type=jnp.float32)]
  transfers between devices with their start and end apart: 2 -> 1, of which waited for: 1 -> 1; matrix products, arithmetic and copies ran while one was open for 5% -> 1% of each run, Pallas kernels for 0% -> 0%
where the time goes in v1:
time: 325 us; the launch traced here: 324 us
  waiting for transfers between devices  223 us (69%)
  blocking collectives  64.4 us (20%)
  other arithmetic  14.6 us (4%)
  local copies, waits for them, and re-layouts  11.4 us (4%)
  starting transfers between devices  5.2 us (2%)
  matrix products  4.84 us (1%)
    all_to_all x1, waiting for transfers between devices, per_device(): lax.all_to_all(jnp.stack([tokens] * lax.axis_size('tp')), 'tp', 0, 0)  223 us
    all_gather x1, blocking collectives, sent_together(): filled = lax.all_gather(both, axis, axis=dim, tiled=True)  47.7 us
    all_to_all x1, blocking collectives, per_device(): lax.all_to_all(cum_gate, 'tp', split_axis=1, concat_axis=2, tiled=True)  16.7 us
    another operation x1, local copies, waits for them, and re-layouts, per_device(): jnp.stack([tokens] * lax.axis_size('tp'))  7.21 us
    reduce_sum x1, other arithmetic, normalize(): jnp.mean(widened * widened, axis=-1, keepdims=True) + 1e-06  7.11 us
  transfers between devices with their start and end apart: 1, of which 1 were waited for; matrix products, arithmetic and copies ran while one was open for 1% of the time, Pallas kernels for 0%

profile of v1, /device:TPU:1, one launch (start us, length us, event | category | flops | bytes accessed | tf_op | source)
XLA Modules:
  0.0 324.3 jit_solution(6760502813533942389)
XLA Ops:
  0.6 0.8 copy.16
  1.4 16.7 %all_to_all.23 = f32[1,32,192]{2,0,1:T(1,128)S(1)} all-to-all(f32[1,32,192]{2,0,1:T(1,128)S(1)} %copy.16), channel_id=1, replica_groups=mesh['sp'=32,'tp'=16] {'tp'}, dimensions={1} | all-to-all | bytes 49152 | tf_op jit(solution)/shard_map/all_to_all | solution.py:29
  18.1 7.2 %stack.2 = bf16[16,1,192,2048]{3,2,1,0:T(8,128)(2,1)} broadcast(bf16[192,2048]{1,0:T(8,128)(2,1)} %bitcast.43), dimensions={2,3} | broadcast | bytes 13369344 | tf_op jit(solution)/shard_map/stack | solution.py:32
  25.4 5.2 %all-to-all-start = ((bf16[16,1,192,2048]{3,2,1,0:T(8,128)(2,1)}), bf16[16,1,192,2048]{3,2,1,0:T(8,128)(2,1)}, u32[]{:S(2)}, u32[]{:S(2)}) async-start(bf16[16,1,192,2048]{3,2,1,0:T(8,128)(2,1)} %stack.2), calls=%async_computation | async-start | bytes 25165824 | tf_op jit(solution)/shard_map/all_to_all | solution.py:32
  30.6 0.5 broadcast.91
  31.1 0.7 reduce.14
  31.7 0.1 reshape.210
  31.9 0.1 reshape.214
  31.9 0.1 bitcast_convert_fusion
  32.0 0.1 multiply_reduce_fusion.1
  32.1 0.1 pad_maximum_fusion
  32.2 47.7 %all_gather.3 = bf16[2048,128]{1,0:T(8,128)(2,1)S(1)} all-gather(bf16[64,128]{1,0:T(8,128)(2,1)S(1)} %pad_maximum_fusion), channel_id=1, replica_groups=mesh['sp'=32,'tp'=16] {'sp'}, dimensions={0}, use_global_device_ids=true | all-gather | bytes 540672 | tf_op jit(solution)/shard_map/all_gather | solution.py:13
  79.9 0.1 reshape.211
  80.0 0.7 all_to_all.20
  80.7 223.2 %all-to-all-done = bf16[16,1,192,2048]{3,2,1,0:T(8,128)(2,1)} async-done(((bf16[16,1,192,2048]{3,2,1,0:T(8,128)(2,1)}), bf16[16,1,192,2048]{3,2,1,0:T(8,128)(2,1)}, u32[]{:S(2)}, u32[]{:S(2)}) %all-to-all-start) | async-done | bytes 12582944 | tf_op jit(solution)/shard_map/all_to_all | solution.py:32
  303.9 7.1 %multiply_reduce_fusion = f32[16,192]{1,0:T(8,128)S(1)} fusion(bf16[16,1,192,2048]{3,2,1,0:T(8,128)(2,1)} %all-to-all-done), kind=kLoop, calls=%fused_computation.2 | loop fusion | flops 18871296 | bytes 12595200 | tf_op jit(solution)/shard_map/reduce_sum | solution.py:19
  311.0 0.1 rsqrt.12
  311.1 6.2 %fusion = bf16[3072,2048]{1,0:T(8,128)(2,1)S(1)} fusion(f32[2048]{0:T(1024)S(1)} %copy-done.2, bf16[16,1,192,2048]{3,2,1,0:T(8,128)(2,1)} %all-to-all-done), kind=kLoop, calls=%fused_computation.1 | loop fusion | flops 18874368 | bytes 25174016 | tf_op jit(solution)/shard_map/convert_element_type | solution.py:20
  317.3 4.3 %fusion.2 = bf16[1,3072,128]{1,2,0:T(8,128)(2,1)S(1)} fusion(bf16[3072,2048]{1,0:T(8,128)(2,1)S(1)} %fusion, bf16[2048,128]{1,0:T(8,128)(2,1)S(1)} %all_gather.3, f32[3072]{0:T(1024)S(1)} %rsqrt.12), kind=kOutput, calls=%fused_computation.5 | convolution fusion | flops 1611399168 | bytes 13905920 | tf_op jit(solution)/shard_map/dot_general | solution.py:36
  321.8 1.2 copy.18
  322.9 0.3 fusion.12
  323.2 0.2 fusion.8
  323.4 0.3 fusion.7
  323.7 0.6 convert_element_type.72
  (19 shorter events, 0.2 us)
Async XLA Ops:
  25.3 5.7 %copy-start.4 = (bf16[1,128]{1,0:T(2,128)(2,1)S(1)}, bf16[1,128]{1,0:T(2,128)(2,1)}, u32[]{:S(2)}) copy-start(bf16[1,128]{1,0:T(2,128)(2,1)} %param.14) | copy-start | bytes 772
  25.4 6.6 %copy-start.3 = (bf16[1,1,128]{2,1,0:T(2,128)(2,1)S(1)}, bf16[1,1,128]{2,1,0:T(2,128)(2,1)}, u32[]{:S(2)}) copy-start(bf16[1,1,128]{2,1,0:T(2,128)(2,1)} %param.15) | copy-start | bytes 772
  25.4 6.8 %copy-start = (bf16[64,64]{1,0:T(8,128)(2,1)S(1)}, bf16[64,64]{1,0:T(8,128)(2,1)}, u32[]{:S(2)}) copy-start(bf16[64,64]{1,0:T(8,128)(2,1)} %param.11) | copy-start | bytes 24580
  25.4 6.8 %copy-start.1 = (bf16[64,64]{1,0:T(8,128)(2,1)S(1)}, bf16[64,64]{1,0:T(8,128)(2,1)}, u32[]{:S(2)}) copy-start(bf16[64,64]{1,0:T(8,128)(2,1)} %param.10) | copy-start | bytes 24580
  25.4 278.5 %all-to-all-start = ((bf16[16,1,192,2048]{3,2,1,0:T(8,128)(2,1)}), bf16[16,1,192,2048]{3,2,1,0:T(8,128)(2,1)}, u32[]{:S(2)}, u32[]{:S(2)}) async-start(bf16[16,1,192,2048]{3,2,1,0:T(8,128)(2,1)} %stack.2), calls=%async_computation | async-start | bytes 25165824 | tf_op jit(solution)/shard_map/all_to_all | solution.py:32
  30.6 280.5 %copy-start.2 = (f32[2048]{0:T(1024)S(1)}, f32[2048]{0:T(1024)}, u32[]{:S(2)}) copy-start(f32[2048]{0:T(1024)} %param.9) | copy-start | bytes 24580
  317.3 5.6 %copy-start.5 = (f32[1,2]{1,0:T(1,128)S(1)}, f32[1,2]{1,0:T(1,128)}, u32[]{:S(2)}) copy-start(f32[1,2]{1,0:T(1,128)} %param.13) | copy-start | bytes 28
